TPU v7x, 256 devices: a 4x2x16 block of a 4x16x16 slice. The times are simulated.
256 devices in a mesh: grp: 2 (over y), sp: 32 (over z, core), tp: 4 (over x).
Axes of the slice: x: 4, y: 2, z: 16, core: 2. Of those that a mesh axis runs over, the one named last changes fastest.
The devices are a block of a 4x16x16 slice.
Arguments:
- query_plain: bfloat16 [10240, 1024], P(('grp', 'sp'), 'tp'), parts along dimension 0, may hold values from -6 to 6
- query_turn: bfloat16 [10240, 512], P(('grp', 'sp'), 'tp'), parts along dimension 0, may hold values from -40 to 40, as said below
- latent: bfloat16 [10240, 512], P(('grp', 'sp')), parts along dimension 0, may hold values from -6 to 6
- key_turn: bfloat16 [10240, 64], P(('grp', 'sp')), parts along dimension 0, may hold values from -40 to 40, as said below
- latent_norm_scale: bfloat16 [512], replicated, may hold values from 0.099609375 to 1.8984375
- plain_key_matrix: bfloat16 [512, 1024], P(None, 'tp'), may hold values from -0.25 to 0.25
- value_matrix: bfloat16 [512, 1024], P(None, 'tp'), may hold values from -0.25 to 0.25
- residual: bfloat16 [10240, 2048], P(('grp', 'sp', 'tp')), parts along dimension 0, may hold values from -6 to 6
- out_weight: bfloat16 [1024, 2048], replicated, may hold values from -6 to 6
- ffn_gain: bfloat16 [2048], replicated, may hold values from 0.099609375 to 1.8984375
- gate_weight: bfloat16 [32, 2048, 1024], P('sp', None, 'tp'), may hold values from -1 to 1
- up_weight: bfloat16 [32, 2048, 1024], P('sp', None, 'tp'), may hold values from -1 to 1
- down_weight: bfloat16 [32, 1024, 2048], P('sp', 'tp'), may hold values from -0.0625 to 0.0625
- routes: int32 [10240, 4], P(('grp', 'sp', 'tp')), parts along dimension 0, may hold values from 0 to 31, all different within a row; in each aligned block of 40 rows (0 to 39, 40 to 79, ...) at most 7 rows name the same one
- route_weights: float32 [10240, 4], P(('grp', 'sp', 'tp')), parts along dimension 0, may hold values from 0.1 to 0.6
Outputs:
- mixed: bfloat16 [10240, 2048], P(('grp', 'sp', 'tp')), parts along dimension 0
There are 2 independent parts, one for each index of `grp`. A program takes and returns all parts, laid end to end along the dimension named above; an argument that names none is the same for every part. Nothing has to cross between parts.
Inputs may be any that keep to these rules, and one draw needn't show every extreme that they name: `query_turn`: in the hidden draw some rows are large. `key_turn`: in the hidden draw some rows are large. `routes`: each row names 4 different experts. In each aligned block of 40 rows (the rows of one device) no expert is named more than 7 times, a bound that some block reaches.
All inputs are finite; a program needn't handle non-finite values.
Results may differ from a plain program's by a relative error of at most 0.015.
Values may be sent and summed in bfloat16 or wider, within the bound.
No kernel may reach another device: no remote copies, remote signals or barrier semaphores. Data moves between devices by JAX's collectives and lax.ppermute only.
A program may use at most 128 MiB of HBM per device.

v0:
```python
import jax
import jax.numpy as jnp
from jax import lax
from jax.sharding import Mesh
from jax.sharding import PartitionSpec as P

PLAIN_HEAD_WIDTH = 128
QK_ROPE = 64
VALUE_WIDTH = 128
GRID_W = 64
SP = ("sp_0", "sp_1")
GRP_SP = ("grp", "sp_0", "sp_1")
GRP_SP_TP = ("grp", "sp_0", "sp_1", "tp")
theta = 10000.0
eps = 1e-06
limit = 7.0
slope = 1.702


def sent_together(arrays, axis, dim, along):
    both = jnp.concatenate(arrays, axis=along)
    result, at, finished = (lax.all_gather(both, axis, axis=dim, tiled=True), 0, [])
    for a in arrays:
        finished.append(lax.slice_in_dim(result, at, at + a.shape[along], axis=along))
        at += a.shape[along]
    return tuple(finished)


def turned_gather(arrays, axis, dims):
    turned = [jnp.moveaxis(a, dim, 0) for a, dim in zip(arrays, dims)]
    both = jnp.concatenate([t.reshape(len(t), -1) for t in turned], axis=1)
    result, at, finished = (lax.all_gather(both, axis, axis=0, tiled=True), 0, [])
    for t, dim in zip(turned, dims):
        share = result[:, at : at + t[0].size].reshape(-1, *t.shape[1:])
        finished.append(jnp.moveaxis(share, 0, dim))
        at += t[0].size
    return tuple(finished)


def cut_along(array, dim, count):
    lengths = array.shape
    blocks = array.reshape(*lengths[:dim], count, lengths[dim] // count, *lengths[dim + 1 :])
    return jnp.moveaxis(blocks, dim, 0)


def laid_out(blocks, dim):
    lengths = list(blocks.shape[1:])
    lengths[dim] *= blocks.shape[0]
    return jnp.moveaxis(blocks, 0, dim).reshape(lengths)


def moved_by_axis(blocks, axes, order):
    inside = blocks.shape[1:]
    result = blocks.reshape(*(lax.axis_size(a) for a in axes), *inside)
    for k in order:
        result = lax.all_to_all(result, axes[k], k, k, tiled=True)
    return result.reshape(-1, *inside)


def exchange_by_chip(array, groups, order, split_dim, concat_dim):
    count = lax.axis_size(groups[0]) * lax.axis_size(groups[1])
    blocks = cut_along(array, split_dim, count)
    return laid_out(moved_by_axis(blocks, groups, order), concat_dim)


def turn(vector, row_shift, col_shift):
    width = vector.shape[-1]
    count = width // 4
    half = width // 2
    freqs = theta ** (-jnp.arange(count, dtype=jnp.float32) / count)
    extra = (1,) * (vector.ndim - 2)
    pieces = []
    for portion, shift in ((vector[..., :half], row_shift), (vector[..., half:], col_shift)):
        angle = (shift.astype(jnp.float32)[:, None] * freqs[None, :]).reshape(
            (shift.shape[0],) + extra + (count,)
        )
        lower = portion[..., :count]
        upper = portion[..., count:]
        pieces.append(
            jnp.concatenate(
                [
                    lower * jnp.cos(angle) - upper * jnp.sin(angle),
                    lower * jnp.sin(angle) + upper * jnp.cos(angle),
                ],
                axis=-1,
            )
        )
    return jnp.concatenate(pieces, axis=-1)


def norm_scale(values, gain):
    wide = values.astype(jnp.float32)
    return (
        wide
        * lax.rsqrt(jnp.mean(wide * wide, axis=-1, keepdims=True) + eps)
        * gain.astype(jnp.float32)
    )


def expert_active(rows, gate_w, up_w):
    gate_pre = jnp.minimum(jnp.dot(rows, gate_w, preferred_element_type=jnp.float32), limit)
    up_pre = jnp.clip(jnp.dot(rows, up_w, preferred_element_type=jnp.float32), -limit, limit)
    return ((up_pre + 1.0) * gate_pre * jax.nn.sigmoid(slope * gate_pre)).astype(jnp.bfloat16)


def expert_whole(rows, gate_w, up_w, down_w, groups):
    active = expert_active(rows, gate_w, up_w)
    piece = down_w.shape[0] // groups
    total = jnp.zeros((rows.shape[0], down_w.shape[1]), jnp.float32)
    for index in range(groups):
        product = jnp.dot(
            active[:, index * piece : (index + 1) * piece],
            down_w[index * piece : (index + 1) * piece],
            preferred_element_type=jnp.float32,
        )
        total = total + product.astype(jnp.bfloat16).astype(jnp.float32)
    return total.astype(jnp.bfloat16)


def on_device(
    query_plain,
    query_turn,
    latent,
    key_turn,
    latent_norm_scale,
    plain_key_matrix,
    value_matrix,
    residual,
    out_weight,
    ffn_gain,
    gate_weight,
    up_weight,
    down_weight,
    routes,
    route_weights,
):
    tok_dev = latent.shape[0]
    heads_dev = query_plain.shape[1] // PLAIN_HEAD_WIDTH
    model_width = residual.shape[1]
    place = lax.axis_index(SP) * tok_dev + jnp.arange(tok_dev, dtype=jnp.int32)
    grid_row = place // GRID_W
    grid_col = place % GRID_W
    normed_latent = norm_scale(latent, latent_norm_scale).astype(jnp.bfloat16)
    key_plain = jnp.dot(normed_latent, plain_key_matrix, preferred_element_type=jnp.float32).astype(
        jnp.bfloat16
    )
    values = jnp.dot(normed_latent, value_matrix, preferred_element_type=jnp.float32).astype(
        jnp.bfloat16
    )
    key_rot = turn(key_turn.astype(jnp.float32), grid_row, grid_col).astype(jnp.bfloat16)
    key_pairs = key_rot.reshape(tok_dev // 2, 2 * QK_ROPE)
    query_rot = turn(
        query_turn.astype(jnp.float32).reshape(tok_dev, heads_dev, QK_ROPE), grid_row, grid_col
    ).astype(jnp.bfloat16)
    plain_query = query_plain.reshape(tok_dev, heads_dev, PLAIN_HEAD_WIDTH)
    scale = (PLAIN_HEAD_WIDTH + QK_ROPE) ** (-0.5)
    most = jnp.full((heads_dev, tok_dev), -jnp.inf, jnp.float32)
    total = jnp.zeros((heads_dev, tok_dev), jnp.float32)
    summed = jnp.zeros((heads_dev, tok_dev, VALUE_WIDTH), jnp.float32)
    piece_keys, piece_values, piece_pairs = (
        *sent_together((key_plain, values), SP, 0, 1),
        lax.all_gather(key_pairs, SP, axis=0, tiled=True),
    )
    count = piece_keys.shape[0]
    piece_rot = piece_pairs.reshape(count, QK_ROPE)
    new_most = []
    new_total = []
    new_summed = []
    for head in range(heads_dev):
        head_keys = piece_keys[:, head * PLAIN_HEAD_WIDTH : (head + 1) * PLAIN_HEAD_WIDTH]
        head_values = piece_values[:, head * VALUE_WIDTH : (head + 1) * VALUE_WIDTH]
        scores = (
            jnp.einsum(
                "qd,kd->qk", plain_query[:, head], head_keys, preferred_element_type=jnp.float32
            )
            + jnp.einsum(
                "qd,kd->qk", query_rot[:, head], piece_rot, preferred_element_type=jnp.float32
            )
        ) * scale
        peak = jnp.max(scores, axis=1)
        factor = jnp.exp(most[head] - peak)
        weights = jnp.exp(scores - peak[:, None])
        new_total.append(total[head] * factor + jnp.sum(weights, axis=1))
        new_summed.append(
            summed[head] * factor[:, None]
            + jnp.dot(weights.astype(jnp.bfloat16), head_values, preferred_element_type=jnp.float32)
        )
        new_most.append(peak)
    total = jnp.stack(new_total)
    summed = jnp.stack(new_summed)
    attended = jnp.transpose((summed / total[..., None]).astype(jnp.bfloat16), (1, 0, 2)).reshape(
        tok_dev, heads_dev * VALUE_WIDTH
    )
    rows_dev = residual.shape[0]
    token_heads = lax.all_to_all(attended, "tp", split_axis=0, concat_axis=1, tiled=True)
    projected = jnp.dot(token_heads, out_weight, preferred_element_type=jnp.float32)
    hidden = (residual.astype(jnp.float32) + projected).astype(jnp.bfloat16)
    normed = norm_scale(hidden, ffn_gain).astype(jnp.bfloat16)
    top_count = routes.shape[1]
    experts_all = lax.axis_size(SP) * gate_weight.shape[0]
    capacity = min(rows_dev, max(2, rows_dev * top_count * 3 // (2 * experts_all)))
    flat_routes = routes.reshape(rows_dev * top_count)
    marks = (flat_routes[:, None] == jnp.arange(experts_all, dtype=jnp.int32)[None, :]).astype(
        jnp.int32
    )
    earlier = jnp.cumsum(marks, axis=0, dtype=jnp.int32) - marks
    slots = jnp.sum(earlier * marks, axis=1, dtype=jnp.int32)
    target = flat_routes * capacity + slots
    chosen = (
        target.reshape(rows_dev, top_count)[None, :, :]
        == jnp.arange(experts_all * capacity, dtype=jnp.int32)[:, None, None]
    )
    dispatch_table = jnp.sum(chosen.astype(jnp.bfloat16), axis=2)
    outgoing = jnp.dot(dispatch_table, normed, preferred_element_type=jnp.float32).astype(
        jnp.bfloat16
    )
    outgoing = outgoing.reshape(experts_all, capacity, model_width)
    gate_w = gate_weight[0]
    up_w = up_weight[0]
    down_w = down_weight[0]
    group = lax.axis_size("tp")
    gate_full, up_full, down_full = turned_gather((gate_w, up_w, down_w), "tp", (1, 1, 0))
    arrived = lax.all_to_all(outgoing, SP, split_axis=0, concat_axis=0, tiled=True)
    result_rows = expert_whole(
        arrived.reshape(experts_all * capacity, model_width), gate_full, up_full, down_full, group
    )
    returned = exchange_by_chip(
        result_rows.reshape(experts_all, capacity, model_width), ("sp_0", "sp_1"), (1, 0), 0, 0
    )
    picked = returned.reshape(experts_all * capacity, model_width)[target]
    picked = picked.reshape(rows_dev, top_count, model_width).astype(jnp.float32)
    return (hidden.astype(jnp.float32) + jnp.sum(route_weights[..., None] * picked, axis=1)).astype(
        jnp.bfloat16
    )


def solution(mesh):
    torus = Mesh(
        mesh.devices.reshape(mesh.shape["grp"], 16, 2, mesh.shape["tp"]),
        ("grp", "sp_0", "sp_1", "tp"),
    )
    placed = (
        P(GRP_SP, "tp"),
        P(GRP_SP, "tp"),
        P(GRP_SP, None),
        P(GRP_SP, None),
        P(),
        P(None, "tp"),
        P(None, "tp"),
        P(GRP_SP_TP, None),
        P(),
        P(),
        P(SP, None, "tp"),
        P(SP, None, "tp"),
        P(SP, "tp", None),
        P(GRP_SP_TP, None),
        P(GRP_SP_TP, None),
    )
    return jax.shard_map(
        on_device, mesh=torus, in_specs=placed, out_specs=P(GRP_SP_TP, None), check_vma=False
    )
```

profile of v0, /device:TPU:34, one launch (start us, length us, event | category | flops | bytes accessed | tf_op | source)
XLA Modules:
  0.0 310.7 jit_solution(7776849853484320127)
XLA Ops:
  6.6 0.8 convert_element_type.119
  7.3 1.0 fusion.74
  8.4 1.2 convolution_convert_fusion.5
  9.6 1.3 convolution_convert_fusion.6
  11.7 1.5 copy.71
  13.8 2.8 pad_maximum_fusion
  17.3 52.1 %all_gather.10 = bf16[2560,128]{1,0:T(8,128)(2,1)S(1)} all-gather(bf16[80,128]{1,0:T(8,128)(2,1)S(1)} %convert_element_type.126), channel_id=1, replica_groups=mesh['grp'=2,'sp_0'=16,'sp_1'=2,'tp'=4] {'sp_0','sp_1'}, dimensions={0}, use_global_device_ids=true | all-gather | bytes 675840 | tf_op jit(solution)/shard_map/all_gather | solution.py:162
  72.1 0.7 fusion.103
  72.8 2.3 fusion.95
  75.1 2.0 fusion.96
  77.1 22.1 %all-gather.3.cloned.1.call-done = bf16[5120,512]{1,0:T(8,128)(2,1)} async-done(((bf16[160,512]{1,0:T(8,128)(2,1)}), bf16[5120,512]{1,0:T(8,128)(2,1)}) %all-gather.3.cloned.1.call-update) | async-done | bytes 5242896 | tf_op jit(solution)/shard_map/all_gather | solution.py:22
  99.2 3.2 %fusion.104 = (f32[160]{0:T(256)S(1)}, f32[160,5120]{1,0:T(8,128)S(1)}) fusion(f32[160,5120]{1,0:T(8,128)} %fusion.95, bf16[160,1,128]{2,1,0:T(2,128)(2,1)S(1)} %copy-done.4, bf16[5120,512]{1,0:T(8,128)(2,1)} %all-gather.3.cloned.1.call-done), kind=kOutput, calls=%fused_computation.135 | convolution fusion | flops 212172640 | bytes 7905920 | tf_op jit(solution)/shard_map/qd,kd->qk/dot_general | solution.py:173
  104.4 0.7 fusion.65
  105.1 0.7 fusion.55
  106.8 4.8 %all-to-all-start = ((bf16[4,40,256]{2,1,0:T(8,128)(2,1)}), bf16[4,40,256]{2,1,0:T(8,128)(2,1)S(1)}, u32[]{:S(2)}, u32[]{:S(2)}) async-start(bf16[4,40,256]{2,1,0:T(8,128)(2,1)} %all_to_all.23), calls=%async_computation | async-start | bytes 163840 | tf_op jit(solution)/shard_map/all_to_all | solution.py:195
  111.6 4.2 %all-to-all-done = bf16[4,40,256]{2,1,0:T(8,128)(2,1)S(1)} async-done(((bf16[4,40,256]{2,1,0:T(8,128)(2,1)}), bf16[4,40,256]{2,1,0:T(8,128)(2,1)S(1)}, u32[]{:S(2)}, u32[]{:S(2)}) %all-to-all-start) | async-done | bytes 81952 | tf_op jit(solution)/shard_map/all_to_all | solution.py:195
  115.8 3.6 %multiply_reduce_fusion.1 = (f32[40]{0:T(128)S(1)}, f32[40,2048]{1,0:T(8,128)S(1)}) fusion(bf16[40,1024]{1,0:T(8,128)(2,1)S(1)} %bitcast.79, bf16[1024,2048]{1,0:T(8,128)(2,1)} %param.23, bf16[40,2048]{1,0:T(8,128)(2,1)S(1)} %copy-done.5), kind=kOutput, calls=%fused_computation.66 | convolution fusion | flops 168263648 | bytes 4767904 | tf_op jit(solution)/shard_map/dot_general | solution.py:196
  120.2 63.2 %all_to_all.34 = bf16[32,7,2048]{2,1,0:T(8,128)(2,1)S(1)} all-to-all(bf16[32,7,2048]{2,1,0:T(8,128)(2,1)S(1)} %reshape.304), channel_id=1, replica_groups=mesh['grp'=2,'sp_0'=16,'sp_1'=2,'tp'=4] {'sp_0','sp_1'}, dimensions={0} | all-to-all | bytes 1835008 | tf_op jit(solution)/shard_map/all_to_all | solution.py:223
  183.7 38.2 %all-gather.5.cloned.1.call-done = bf16[1024,6144]{1,0:T(8,128)(2,1)} async-done(((bf16[256,6144]{1,0:T(8,128)(2,1)}), bf16[1024,6144]{1,0:T(8,128)(2,1)}) %all-gather.5.cloned.1.call-update) | async-done | bytes 12582928 | tf_op jit(solution)/shard_map/all_gather | solution.py:32
  221.9 3.6 %fusion.44 = f32[224,1024]{1,0:T(8,128)S(1)} fusion(bf16[224,2048]{1,0:T(8,128)(2,1)S(1)} %reshape.305, bf16[1024,6144]{1,0:T(8,128)(2,1)} %all-gather.5.cloned.1.call-done), kind=kOutput, calls=%fused_computation.47 | convolution fusion | flops 939753472 | bytes 6029312 | tf_op jit(solution)/shard_map/dot_general | solution.py:101
  225.5 3.7 %fusion.47 = bf16[224,1024]{1,0:T(8,128)(2,1)S(1)} fusion(f32[224,1024]{1,0:T(8,128)S(1)} %fusion.44, bf16[224,2048]{1,0:T(8,128)(2,1)S(1)} %reshape.305, bf16[1024,6144]{1,0:T(8,128)(2,1)} %all-gather.5.cloned.1.call-done), kind=kOutput, calls=%fused_computation.48 | convolution fusion | flops 941588480 | bytes 6488064 | tf_op jit(solution)/shard_map/dot_general | solution.py:102
  229.2 1.6 fusion.19
  230.9 1.6 fusion.18
  232.5 1.6 fusion.16
  234.1 1.6 fusion.14
  236.7 4.5 %all_to_all.35 = bf16[16,2,1,7,2048]{4,0,3,2,1:T(8,128)(2,1)S(1)} all-to-all(bf16[16,2,1,7,2048]{4,0,3,2,1:T(8,128)(2,1)S(1)} %copy.72), channel_id=1, replica_groups=mesh['grp'=2,'sp_0'=16,'sp_1'=2,'tp'=4] {'sp_1'}, dimensions={1} | all-to-all | bytes 1835008 | tf_op jit(solution)/shard_map/all_to_all | solution.py:56
  241.2 1.9 copy.73
  243.1 12.4 %all-to-all-start.3 = ((bf16[16,2,1,7,2048]{4,1,3,2,0:T(2,128)(2,1)}), bf16[16,2,1,7,2048]{4,1,3,2,0:T(2,128)(2,1)S(1)}, u32[]{:S(2)}, u32[]{:S(2)}) async-start(bf16[16,2,1,7,2048]{4,1,3,2,0:T(2,128)(2,1)} %copy.73), calls=%async_computation.3 | async-start | bytes 1835008 | tf_op jit(solution)/shard_map/all_to_all | solution.py:56
  255.7 44.4 %all-to-all-done.3 = bf16[16,2,1,7,2048]{4,1,3,2,0:T(2,128)(2,1)S(1)} async-done(((bf16[16,2,1,7,2048]{4,1,3,2,0:T(2,128)(2,1)}), bf16[16,2,1,7,2048]{4,1,3,2,0:T(2,128)(2,1)S(1)}, u32[]{:S(2)}, u32[]{:S(2)}) %all-to-all-start.3) | async-done | bytes 917536 | tf_op jit(solution)/shard_map/all_to_all | solution.py:56
  300.8 1.0 gather_fusion
  302.2 0.9 multiply_reduce_fusion
  303.2 0.7 add_convert_fusion
  (89 shorter events, 10.8 us)
Async XLA Ops:
  6.5 1.8 copy-start
  6.6 6.6 %copy-start.3 = (bf16[1,2048,256]{2,1,0:T(8,128)(2,1)S(1)}, bf16[1,2048,256]{2,1,0:T(8,128)(2,1)}, u32[]{:S(2)}) copy-start(bf16[1,2048,256]{2,1,0:T(8,128)(2,1)} %param.25) | copy-start | bytes 3145732
  6.6 92.6 %all-gather.3.cloned.1.call-start = ((), (), s32[]{:S(2)}) async-start(), calls=%async_computation.4 | async-start | bytes 5406720 | tf_op jit(solution)/shard_map/all_gather | solution.py:22
  11.6 210.3 %all-gather.5.cloned.1.call-start = ((), (), s32[]{:S(2)}) async-start(), calls=%async_computation.5 | async-start | bytes 15728640 | tf_op jit(solution)/shard_map/all_gather | solution.py:32
  13.8 2.9 copy-start.9
  16.7 53.2 %copy-start.8 = (bf16[160,128]{1,0:T(8,128)(2,1)S(1)}, bf16[160,128]{1,0:T(8,128)(2,1)}, u32[]{:S(2)}) copy-start(bf16[160,128]{1,0:T(8,128)(2,1)} %param.16) | copy-start | bytes 122884
  16.7 53.3 %copy-start.7 = (bf16[160,256]{1,0:T(8,128)(2,1)S(1)}, bf16[160,256]{1,0:T(8,128)(2,1)}, u32[]{:S(2)}) copy-start(bf16[160,256]{1,0:T(8,128)(2,1)} %param.15) | copy-start | bytes 245764
  16.7 53.4 %copy-start.11 = (s32[40,4]{0,1:T(4,128)S(1)}, s32[40,4]{0,1:T(4,128)}, u32[]{:S(2)}) copy-start(s32[40,4]{0,1:T(4,128)} %param.28) | copy-start | bytes 1924
  16.7 55.3 %copy-start.10 = (bf16[2048]{0:T(1024)(128)(2,1)S(1)}, bf16[2048]{0:T(1024)(128)(2,1)}, u32[]{:S(2)}) copy-start(bf16[2048]{0:T(1024)(128)(2,1)} %param.24) | copy-start | bytes 12292
  69.8 3.0 copy-start.2
  75.1 24.1 %copy-start.4 = (bf16[160,1,128]{2,1,0:T(2,128)(2,1)S(1)}, bf16[160,1,128]{2,1,0:T(2,128)(2,1)}, u32[]{:S(2)}) copy-start(bf16[160,1,128]{2,1,0:T(2,128)(2,1)} %get-tuple-element.12) | copy-start | bytes 122884
  99.2 3.8 %slice-start = ((s8[5242880]{0:T(1024)(128)(4,1)}), s8[4194304]{0:T(1024)(128)(4,1)S(1)}, s32[]{:S(2)}) async-start(s8[5242880]{0:T(1024)(128)(4,1)} %bitcast.73), calls=%async_computation.6 | async-start | bytes 8388608
  99.2 3.9 %slice-start.1 = ((s8[5242880]{0:T(1024)(128)(4,1)}), s8[1048576]{0:T(1024)(128)(4,1)S(1)}, s32[]{:S(2)}) async-start(s8[5242880]{0:T(1024)(128)(4,1)} %bitcast.73), calls=%async_computation.7 | async-start | bytes 2097152
  105.1 10.7 %copy-start.5 = (bf16[40,2048]{1,0:T(8,128)(2,1)S(1)}, bf16[40,2048]{1,0:T(8,128)(2,1)}, u32[]{:S(2)}) copy-start(bf16[40,2048]{1,0:T(8,128)(2,1)} %param.22) | copy-start | bytes 491524
  106.8 9.0 %all-to-all-start = ((bf16[4,40,256]{2,1,0:T(8,128)(2,1)}), bf16[4,40,256]{2,1,0:T(8,128)(2,1)S(1)}, u32[]{:S(2)}, u32[]{:S(2)}) async-start(bf16[4,40,256]{2,1,0:T(8,128)(2,1)} %all_to_all.23), calls=%async_computation | async-start | bytes 163840 | tf_op jit(solution)/shard_map/all_to_all | solution.py:195
  236.1 19.3 %copy-start.6 = (s32[40,4]{1,0:T(8,128)S(1)}, s32[40,4]{1,0:T(8,128)}, u32[]{:S(2)}) copy-start(s32[40,4]{1,0:T(8,128)} %get-tuple-element.19) | copy-start | bytes 1924
  236.1 19.4 %copy-start.12 = (f32[40,4]{0,1:T(4,128)S(1)}, f32[40,4]{0,1:T(4,128)}, u32[]{:S(2)}) copy-start(f32[40,4]{0,1:T(4,128)} %param.29) | copy-start | bytes 1924
  243.1 57.0 %all-to-all-start.3 = ((bf16[16,2,1,7,2048]{4,1,3,2,0:T(2,128)(2,1)}), bf16[16,2,1,7,2048]{4,1,3,2,0:T(2,128)(2,1)S(1)}, u32[]{:S(2)}, u32[]{:S(2)}) async-start(bf16[16,2,1,7,2048]{4,1,3,2,0:T(2,128)(2,1)} %copy.73), calls=%async_computation.3 | async-start | bytes 1835008 | tf_op jit(solution)/shard_map/all_to_all | solution.py:56
  300.8 3.1 %copy-start.1 = (bf16[512,256]{1,0:T(8,128)(2,1)S(1)}, bf16[512,256]{1,0:T(8,128)(2,1)}, u32[]{:S(2)}) copy-start(bf16[512,256]{1,0:T(8,128)(2,1)} %param.21) | copy-start | bytes 786436
Sparse Core Ops, SparseCore 0:
  11.7 87.4 all-gather.2
  101.0 120.8 all-gather.4
where the time goes:
time: 312 us; the launch traced here: 311 us
  blocking collectives  120 us (38%)
  waiting for transfers between devices  109 us (35%)
  matrix products  29.9 us (10%)
  starting transfers between devices  17.2 us (6%)
  between operations  13.9 us (4%)
  local copies, waits for them, and re-layouts  10.8 us (3%)
  other arithmetic  10.1 us (3%)
    all_to_all x1, blocking collectives, on_device(): lax.all_to_all(outgoing, SP, split_axis=0, concat_axis=0, tiled=True)  63.2 us
    all_gather x1, blocking collectives, on_device(): lax.all_gather(key_pairs, SP, axis=0, tiled=True)  52.1 us
    all_to_all x1, waiting for transfers between devices, moved_by_axis(): result = lax.all_to_all(result, axes[k], k, k, tiled=True)  44.4 us
    all_gather x1, waiting for transfers between devices, turned_gather(): lax.all_gather(both, axis, axis=0, tiled=True)  38.2 us
    all_gather x1, waiting for transfers between devices, sent_together(): lax.all_gather(both, axis, axis=dim, tiled=True)  22.1 us
    all_to_all x1, starting transfers between devices, moved_by_axis(): result = lax.all_to_all(result, axes[k], k, k, tiled=True)  12.4 us
    dot_general x4, matrix products, expert_whole(): jnp.dot(active[:, index * piece:(index + 1) * piece], down_w[index * piec...  6.55 us
  transfers between devices with their start and end apart: 4, of which 4 were waited for; matrix products, arithmetic and copies ran while one was open for 8% of the time, Pallas kernels for 0%

commit v1 on v0

--- a/solution.py
+++ b/solution.py
@@ -29,7 +29,13 @@
 def turned_gather(arrays, axis, dims):
     turned = [jnp.moveaxis(a, dim, 0) for a, dim in zip(arrays, dims)]
     both = jnp.concatenate([t.reshape(len(t), -1) for t in turned], axis=1)
-    result, at, finished = (lax.all_gather(both, axis, axis=0, tiled=True), 0, [])
+    result, at, finished = (
+        jnp.concatenate(
+            lax.all_to_all(jnp.stack([both] * lax.axis_size(axis)), axis, 0, 0), axis=0
+        ),
+        0,
+        [],
+    )
     for t, dim in zip(turned, dims):
         share = result[:, at : at + t[0].size].reshape(-1, *t.shape[1:])
         finished.append(jnp.moveaxis(share, 0, dim))

time: 312 us -> 420 us (1.35)
  waiting for transfers between devices: 109 us -> 263 us
  blocking collectives: 120 us -> 55.8 us
  local copies, waits for them, and re-layouts: 10.8 us -> 20.4 us
  starting transfers between devices: 17.2 us -> 25.3 us
    all_to_all x0 -> x2, waiting for transfers between devices: none -> 187 us  [the longest x1 136 us: turned_gather(): lax.all_to_all(jnp.stack([both] * lax.axis_size(axis)), axis, 0, 0)]
    all_to_all x1 -> x0, blocking collectives: 63.2 us -> none  [on_device(): lax.all_to_all(outgoing, SP, split_axis=0, concat_axis=0, tiled=True)]
    all_gather x1 -> x0, waiting for transfers between devices: 38.2 us -> none  [turned_gather(): lax.all_gather(both, axis, axis=0, tiled=True)]
    all_to_all x0 -> x2, starting transfers between devices: none -> 15.7 us  [the longest x1 7.92 us: turned_gather(): lax.all_to_all(jnp.stack([both] * lax.axis_size(axis)), axis, 0, 0)]
    all_to_all x1, starting transfers between devices: 12.4 us -> 4.07 us  [moved_by_axis(): result = lax.all_to_all(result, axes[k], k, k, tiled=True)]
    another operation x1 -> x2, local copies, waits for them, and re-layouts: 0.01 us -> 6.04 us  [the longest x1 6.03 us: turned_gather(): jnp.stack([both] * lax.axis_size(axis))]
    all_gather x1, waiting for transfers between devices: 22.1 us -> 26.5 us  [sent_together(): lax.all_gather(both, axis, axis=dim, tiled=True)]
  transfers between devices with their start and end apart: 4 -> 5, of which waited for: 4 -> 5; matrix products, arithmetic and copies ran while one was open for 8% -> 4% of each run, Pallas kernels for 0% -> 0%
where the time goes in v1:
time: 420 us; the launch traced here: 418 us
  waiting for transfers between devices  263 us (63%)
  blocking collectives  55.8 us (13%)
  matrix products  29.5 us (7%)
  starting transfers between devices  25.3 us (6%)
  local copies, waits for them, and re-layouts  20.4 us (5%)
  between operations  13.9 us (3%)
  other arithmetic  10 us (2%)
    all_to_all x1, waiting for transfers between devices, turned_gather(): lax.all_to_all(jnp.stack([both] * lax.axis_size(axis)), axis, 0, 0)  136 us
    all_gather x1, blocking collectives, on_device(): lax.all_gather(key_pairs, SP, axis=0, tiled=True)  51.3 us
    all_to_all x1, waiting for transfers between devices, on_device(): lax.all_to_all(outgoing, SP, split_axis=0, concat_axis=0, tiled=True)  50.5 us
    all_to_all x1, waiting for transfers between devices, moved_by_axis(): result = lax.all_to_all(result, axes[k], k, k, tiled=True)  45.5 us
    all_gather x1, waiting for transfers between devices, sent_together(): lax.all_gather(both, axis, axis=dim, tiled=True)  26.5 us
  transfers between devices with their start and end apart: 5, of which 5 were waited for; matrix products, arithmetic and copies ran while one was open for 4% of the time, Pallas kernels for 0%

profile of v1, /device:TPU:34, one launch (start us, length us, event | category | flops | bytes accessed | tf_op | source)
XLA Modules:
  0.0 418.1 jit_solution(3674537627970618317)
XLA Ops:
  7.4 1.0 fusion.74
  8.5 1.2 convolution_convert_fusion.5
  9.6 1.3 convolution_convert_fusion.6
  12.9 51.3 %all_gather.7 = bf16[2560,128]{1,0:T(8,128)(2,1)S(1)} all-gather(bf16[80,128]{1,0:T(8,128)(2,1)S(1)} %convert_element_type.126), channel_id=1, replica_groups=mesh['grp'=2,'sp_0'=16,'sp_1'=2,'tp'=4] {'sp_0','sp_1'}, dimensions={0}, use_global_device_ids=true | all-gather | bytes 675840 | tf_op jit(solution)/shard_map/all_gather | solution.py:168
  67.7 2.3 fusion.95
  70.0 2.0 fusion.96
  72.0 26.5 %all-gather.2.cloned.1.call-done = bf16[5120,512]{1,0:T(8,128)(2,1)} async-done(((bf16[160,512]{1,0:T(8,128)(2,1)}), bf16[5120,512]{1,0:T(8,128)(2,1)}) %all-gather.2.cloned.1.call-update) | async-done | bytes 5242896 | tf_op jit(solution)/shard_map/all_gather | solution.py:22
  98.5 3.2 fusion.104
  106.1 5.5 %all-to-all-start = ((bf16[4,40,256]{2,1,0:T(8,128)(2,1)}), bf16[4,40,256]{2,1,0:T(8,128)(2,1)S(1)}, u32[]{:S(2)}, u32[]{:S(2)}) async-start(bf16[4,40,256]{2,1,0:T(8,128)(2,1)} %all_to_all.26), calls=%async_computation | async-start | bytes 163840 | tf_op jit(solution)/shard_map/all_to_all | solution.py:201
  111.7 4.2 all-to-all-done
  115.9 3.1 multiply_reduce_fusion.1
  120.2 1.3 reshape.309
  121.5 7.8 %all-to-all-start.1 = ((bf16[32,7,2048]{2,1,0:T(8,128)(2,1)}), bf16[32,7,2048]{2,1,0:T(8,128)(2,1)}, u32[]{:S(2)}, u32[]{:S(2)}) async-start(bf16[32,7,2048]{2,1,0:T(8,128)(2,1)} %reshape.309), calls=%async_computation.1 | async-start | bytes 2097152 | tf_op jit(solution)/shard_map/all_to_all | solution.py:229
  129.3 1.4 copy.71
  130.7 1.4 copy.70
  132.1 2.0 pad_maximum_fusion
  134.1 50.5 %all-to-all-done.1 = bf16[32,7,2048]{2,1,0:T(8,128)(2,1)} async-done(((bf16[32,7,2048]{2,1,0:T(8,128)(2,1)}), bf16[32,7,2048]{2,1,0:T(8,128)(2,1)}, u32[]{:S(2)}, u32[]{:S(2)}) %all-to-all-start.1) | async-done | bytes 917536 | tf_op jit(solution)/shard_map/all_to_all | solution.py:229
  184.6 6.0 %stack.25 = bf16[4,256,6144]{2,1,0:T(8,128)(2,1)} broadcast(bf16[256,6144]{1,0:T(8,128)(2,1)S(1)} %pad_maximum_fusion), dimensions={1,2} | broadcast | bytes 15728640 | tf_op jit(solution)/shard_map/stack | solution.py:34
  190.7 7.9 %all-to-all-start.2 = ((bf16[4,256,6144]{2,1,0:T(8,128)(2,1)}), bf16[4,256,6144]{2,1,0:T(8,128)(2,1)}, u32[]{:S(2)}, u32[]{:S(2)}) async-start(bf16[4,256,6144]{2,1,0:T(8,128)(2,1)} %stack.25), calls=%async_computation.2 | async-start | bytes 25165824 | tf_op jit(solution)/shard_map/all_to_all | solution.py:34
  198.6 1.5 reshape.310
  200.1 136.3 %all-to-all-done.2 = bf16[4,256,6144]{2,1,0:T(8,128)(2,1)} async-done(((bf16[4,256,6144]{2,1,0:T(8,128)(2,1)}), bf16[4,256,6144]{2,1,0:T(8,128)(2,1)}, u32[]{:S(2)}, u32[]{:S(2)}) %all-to-all-start.2) | async-done | bytes 12582944 | tf_op jit(solution)/shard_map/all_to_all | solution.py:34
  336.4 3.6 fusion.44
  340.0 3.7 fusion.47
  343.7 1.6 fusion.19
  345.4 1.6 fusion.18
  347.0 1.6 fusion.16
  348.7 1.6 fusion.14
  351.2 4.5 %all_to_all.39 = bf16[16,2,1,7,2048]{4,0,3,2,1:T(8,128)(2,1)S(1)} all-to-all(bf16[16,2,1,7,2048]{4,0,3,2,1:T(8,128)(2,1)S(1)} %copy.72), channel_id=1, replica_groups=mesh['grp'=2,'sp_0'=16,'sp_1'=2,'tp'=4] {'sp_1'}, dimensions={1} | all-to-all | bytes 1835008 | tf_op jit(solution)/shard_map/all_to_all | solution.py:62
  355.7 1.9 copy.73
  357.6 4.1 all-to-all-start.4
  361.9 45.5 %all-to-all-done.4 = bf16[16,2,1,7,2048]{4,1,3,2,0:T(2,128)(2,1)S(1)} async-done(((bf16[16,2,1,7,2048]{4,1,3,2,0:T(2,128)(2,1)}), bf16[16,2,1,7,2048]{4,1,3,2,0:T(2,128)(2,1)S(1)}, u32[]{:S(2)}, u32[]{:S(2)}) %all-to-all-start.4) | async-done | bytes 917536 | tf_op jit(solution)/shard_map/all_to_all | solution.py:62
  408.1 1.0 gather_fusion
  (94 shorter events, 15.6 us)
Async XLA Ops:
  6.5 1.9 copy-start
  6.6 58.2 %copy-start.11 = (bf16[160,128]{1,0:T(8,128)(2,1)S(1)}, bf16[160,128]{1,0:T(8,128)(2,1)}, u32[]{:S(2)}) copy-start(bf16[160,128]{1,0:T(8,128)(2,1)} %param.16) | copy-start | bytes 122884
  6.6 58.3 %copy-start.10 = (bf16[160,256]{1,0:T(8,128)(2,1)S(1)}, bf16[160,256]{1,0:T(8,128)(2,1)}, u32[]{:S(2)}) copy-start(bf16[160,256]{1,0:T(8,128)(2,1)} %param.15) | copy-start | bytes 245764
  6.6 58.4 %copy-start.13 = (s32[40,4]{0,1:T(4,128)S(1)}, s32[40,4]{0,1:T(4,128)}, u32[]{:S(2)}) copy-start(s32[40,4]{0,1:T(4,128)} %param.28) | copy-start | bytes 1924
  6.6 60.4 %copy-start.12 = (bf16[2048]{0:T(1024)(128)(2,1)S(1)}, bf16[2048]{0:T(1024)(128)(2,1)}, u32[]{:S(2)}) copy-start(bf16[2048]{0:T(1024)(128)(2,1)} %param.24) | copy-start | bytes 12292
  6.6 92.0 %all-gather.2.cloned.1.call-start = ((), (), s32[]{:S(2)}) async-start(), calls=%async_computation.5 | async-start | bytes 5406720 | tf_op jit(solution)/shard_map/all_gather | solution.py:22
  64.7 3.0 copy-start.2
  70.0 28.5 %copy-start.7 = (bf16[160,1,128]{2,1,0:T(2,128)(2,1)S(1)}, bf16[160,1,128]{2,1,0:T(2,128)(2,1)}, u32[]{:S(2)}) copy-start(bf16[160,1,128]{2,1,0:T(2,128)(2,1)} %get-tuple-element.12) | copy-start | bytes 122884
  98.5 3.8 slice-start
  98.5 3.9 slice-start.1
  104.5 11.4 %copy-start.8 = (bf16[40,2048]{1,0:T(8,128)(2,1)S(1)}, bf16[40,2048]{1,0:T(8,128)(2,1)}, u32[]{:S(2)}) copy-start(bf16[40,2048]{1,0:T(8,128)(2,1)} %param.22) | copy-start | bytes 491524
  106.1 9.8 %all-to-all-start = ((bf16[4,40,256]{2,1,0:T(8,128)(2,1)}), bf16[4,40,256]{2,1,0:T(8,128)(2,1)S(1)}, u32[]{:S(2)}, u32[]{:S(2)}) async-start(bf16[4,40,256]{2,1,0:T(8,128)(2,1)} %all_to_all.26), calls=%async_computation | async-start | bytes 163840 | tf_op jit(solution)/shard_map/all_to_all | solution.py:201
  119.0 0.7 copy-start.3
  119.1 10.2 %copy-start.5 = (bf16[1,2048,256]{2,1,0:T(8,128)(2,1)S(1)}, bf16[1,2048,256]{2,1,0:T(8,128)(2,1)}, u32[]{:S(2)}) copy-start(bf16[1,2048,256]{2,1,0:T(8,128)(2,1)} %param.26) | copy-start | bytes 3145732
  120.2 10.5 %copy-start.6 = (bf16[1,2048,256]{2,1,0:T(8,128)(2,1)S(1)}, bf16[1,2048,256]{2,1,0:T(8,128)(2,1)}, u32[]{:S(2)}) copy-start(bf16[1,2048,256]{2,1,0:T(8,128)(2,1)} %param.25) | copy-start | bytes 3145732
  121.5 63.1 %all-to-all-start.1 = ((bf16[32,7,2048]{2,1,0:T(8,128)(2,1)}), bf16[32,7,2048]{2,1,0:T(8,128)(2,1)}, u32[]{:S(2)}, u32[]{:S(2)}) async-start(bf16[32,7,2048]{2,1,0:T(8,128)(2,1)} %reshape.309), calls=%async_computation.1 | async-start | bytes 2097152 | tf_op jit(solution)/shard_map/all_to_all | solution.py:229
  190.7 145.7 %all-to-all-start.2 = ((bf16[4,256,6144]{2,1,0:T(8,128)(2,1)}), bf16[4,256,6144]{2,1,0:T(8,128)(2,1)}, u32[]{:S(2)}, u32[]{:S(2)}) async-start(bf16[4,256,6144]{2,1,0:T(8,128)(2,1)} %stack.25), calls=%async_computation.2 | async-start | bytes 25165824 | tf_op jit(solution)/shard_map/all_to_all | solution.py:34
  350.6 11.1 %copy-start.9 = (s32[40,4]{1,0:T(8,128)S(1)}, s32[40,4]{1,0:T(8,128)}, u32[]{:S(2)}) copy-start(s32[40,4]{1,0:T(8,128)} %get-tuple-element.19) | copy-start | bytes 1924
  350.6 11.2 %copy-start.14 = (f32[40,4]{0,1:T(4,128)S(1)}, f32[40,4]{0,1:T(4,128)}, u32[]{:S(2)}) copy-start(f32[40,4]{0,1:T(4,128)} %param.29) | copy-start | bytes 1924
  357.6 49.9 %all-to-all-start.4 = ((bf16[16,2,1,7,2048]{4,1,3,2,0:T(2,128)(2,1)}), bf16[16,2,1,7,2048]{4,1,3,2,0:T(2,128)(2,1)S(1)}, u32[]{:S(2)}, u32[]{:S(2)}) async-start(bf16[16,2,1,7,2048]{4,1,3,2,0:T(2,128)(2,1)} %copy.73), calls=%async_computation.4 | async-start | bytes 1835008 | tf_op jit(solution)/shard_map/all_to_all | solution.py:62
  408.1 3.1 copy-start.1
  409.2 1.4 copy-start.4
Sparse Core Ops, SparseCore 0:
  11.8 86.7 all-gather.1
